TPU v7x, 32 devices: a whole 2x2x4 slice. The times are simulated.
32 devices in a mesh: kv: 8 (over z, core), tp: 4 (over y, x).
Axes of the slice: x: 2, y: 2, z: 4, core: 2. Of those that a mesh axis runs over, the one named last changes fastest.
Arguments:
- tokens: bfloat16 [16, 2048], P(None, 'kv'), may hold values from -8 to 8
- lengths: int32 [16], replicated, may hold values from 1 to 3072, 12288 in all
- latent_cache: bfloat16 [16, 3072, 256], P(None, ('kv', 'tp')), may hold values from -10 to 10
- rope_cache: bfloat16 [16, 3072, 32], P(None, ('kv', 'tp')), may hold values from -2000 to 2000
- gain_in: bfloat16 [2048], P('kv'), may hold values from 0.099609375 to 1.8984375
- w_down_q: bfloat16 [2048, 512], P('kv'), may hold values from -0.125 to 0.125
- w_down_kv: bfloat16 [2048, 256], P('kv'), may hold values from -0.125 to 0.125
- w_rope_key: bfloat16 [2048, 32], P('kv'), may hold values from -0.125 to 0.125
- gain_q: bfloat16 [512], replicated, may hold values from 0.099609375 to 1.8984375
- w_up_qn: bfloat16 [512, 16, 64], replicated, may hold values from -0.25 to 0.25
- w_up_qr: bfloat16 [512, 16, 32], replicated, may hold values from -0.25 to 0.25
- gain_kv: bfloat16 [256], replicated, may hold values from 0.099609375 to 1.8984375
- w_key_up: bfloat16 [256, 16, 64], replicated, may hold values from -0.375 to 0.375
- w_value_up: bfloat16 [256, 16, 64], replicated, may hold values from -0.375 to 0.375
- w_attn_out: bfloat16 [16, 64, 2048], P('tp', None, 'kv'), may hold values from -0.1875 to 0.1875
- gain_mid: bfloat16 [2048], P('kv'), may hold values from 0.099609375 to 1.8984375
- w_ff_in: bfloat16 [2048, 8192], P('kv', 'tp'), may hold values from -0.125 to 0.125
- w_ff_out: bfloat16 [8192, 2048], P('tp', 'kv'), may hold values from -0.0625 to 0.0625
Outputs:
- mixed: bfloat16 [16, 2048], P(None, 'kv')
- new_latent: bfloat16 [16, 256], replicated
- new_rope_key: bfloat16 [16, 32], replicated
Inputs may be any that keep to these rules, and one draw needn't show every extreme that they name: `lengths`: each sequence's live cache positions; one sequence fills the whole cache.
All inputs are finite; a program needn't handle non-finite values.
Results may differ from a plain program's by a relative error of at most 0.012.
Values sent between devices are 32-bit elements; how exact they have to be, the bound alone decides.
No kernel may reach another device: no remote copies, remote signals or barrier semaphores. Data moves between devices by JAX's collectives and lax.ppermute only.
A program may use at most 64 MiB of HBM per device.

v0:
```python
import jax
import jax.numpy as jnp
from jax import lax
from jax.sharding import PartitionSpec as P

D = 2048
NOPE = 64
ROPE = 32
EPS = 1e-06


def combined_all(part, axis, combine):
    gathered = jax.tree.map(lambda a: lax.all_gather(a, axis), part)

    def take(source):
        return jax.tree.map(lambda a: lax.dynamic_index_in_dim(a, source, 0, False), gathered)

    return lax.fori_loop(
        1, lax.axis_size(axis), lambda source, state: combine(state, take(source)), take(0)
    )


def rotate(values, positions):
    half = values.shape[-1] // 2
    inverse = 10000.0 ** (-jnp.arange(half, dtype=jnp.float32) / half)
    angle = positions.astype(jnp.float32)[:, None, None] * inverse[None, None, :]
    first = values[..., :half]
    second = values[..., half:]
    return jnp.concatenate(
        [
            first * jnp.cos(angle) - second * jnp.sin(angle),
            second * jnp.cos(angle) + first * jnp.sin(angle),
        ],
        axis=-1,
    )


def rms_scaled(values, gain):
    return (
        values
        * lax.rsqrt(jnp.mean(values * values, axis=-1, keepdims=True) + EPS)
        * gain.astype(jnp.float32)
    )


def combine(earlier, later):
    top_a, total_a, acc_a = earlier
    top_b, total_b, acc_b = later
    top = jnp.maximum(top_a, top_b)
    fade_a = jnp.exp(top_a - top)
    fade_b = jnp.exp(top_b - top)
    return (
        top,
        total_a * fade_a + total_b * fade_b,
        acc_a * fade_a[..., None] + acc_b * fade_b[..., None],
    )


def fold_sources(parts):
    tops, totals, accs = parts
    top = jnp.max(tops, axis=0)
    fade = jnp.exp(tops - top[None])
    return (top, jnp.sum(totals * fade, axis=0), jnp.sum(accs * fade[..., None], axis=0))


def per_device(
    tokens,
    lengths,
    latent_cache,
    rope_cache,
    gain_in,
    w_down_q,
    w_down_kv,
    w_rope_key,
    gain_q,
    w_up_qn,
    w_up_qr,
    gain_kv,
    w_key_up,
    w_value_up,
    w_attn_out,
    gain_mid,
    w_ff_in,
    w_ff_out,
):
    f32 = jnp.float32
    bf16 = jnp.bfloat16
    highest = lax.Precision.HIGHEST
    scale = (NOPE + ROPE) ** (-0.5)
    resid = tokens.astype(f32)
    scaled_in = (resid * gain_in.astype(f32)).astype(bf16)
    part_q = jnp.dot(scaled_in, w_down_q, preferred_element_type=f32)
    part_kv = jnp.dot(scaled_in, w_down_kv, preferred_element_type=f32)
    part_rope = jnp.dot(scaled_in, w_rope_key, preferred_element_type=f32)
    square_in = jnp.sum(resid * resid, axis=1)
    sum_q, sum_kv, sum_rope, total_in = lax.psum((part_q, part_kv, part_rope, square_in), "kv")
    inv_in = lax.rsqrt(total_in / D + EPS)[:, None]
    query_latent = rms_scaled(inv_in * sum_q, gain_q).astype(bf16)
    new_latent = rms_scaled(inv_in * sum_kv, gain_kv).astype(bf16)
    new_rope_key = rotate((inv_in * sum_rope)[:, None, :], lengths)[:, 0, :].astype(bf16)
    query_nope = jnp.einsum(
        "bc,chd->bhd", query_latent, w_up_qn, preferred_element_type=f32
    ).astype(bf16)
    query_rope = rotate(
        jnp.einsum("bc,chr->bhr", query_latent, w_up_qr, preferred_element_type=f32), lengths
    ).astype(bf16)
    query_cache = jnp.einsum(
        "bhd,khd->bhk", query_nope, w_key_up, preferred_element_type=f32
    ).astype(bf16)
    rows = latent_cache.shape[1]
    positions = lax.axis_index(("kv", "tp")) * rows + jnp.arange(rows, dtype=jnp.int32)
    live = (positions[None, :] < lengths[:, None])[:, None, :]
    scores = (
        jnp.einsum("bhk,blk->bhl", query_cache, latent_cache, preferred_element_type=f32)
        + jnp.einsum("bhr,blr->bhl", query_rope, rope_cache, preferred_element_type=f32)
    ) * scale
    scores = jnp.where(live, scores, -1e30)
    top = jnp.max(scores, axis=2)
    weights = jnp.where(live, jnp.exp(scores - top[:, :, None]), 0.0)
    total = jnp.sum(weights, axis=2)
    acc = jnp.einsum("bhl,blk->bhk", weights.astype(bf16), latent_cache, preferred_element_type=f32)
    heads_dev = w_attn_out.shape[0]
    first_head = lax.axis_index("tp") * heads_dev
    own_value_up = lax.dynamic_slice_in_dim(w_value_up, first_head, heads_dev, 1).astype(f32)
    own_cache_q = lax.dynamic_slice_in_dim(query_cache, first_head, heads_dev, 1)
    own_rope_q = lax.dynamic_slice_in_dim(query_rope, first_head, heads_dev, 1)
    self_score = (
        jnp.einsum("bhk,bk->bh", own_cache_q, new_latent, preferred_element_type=f32)
        + jnp.einsum("bhr,br->bh", own_rope_q, new_rope_key, preferred_element_type=f32)
    ) * scale
    top, total, acc = fold_sources(
        (
            lax.all_to_all(top[None], "tp", split_axis=2, concat_axis=0, tiled=True),
            lax.all_to_all(total[None], "tp", split_axis=2, concat_axis=0, tiled=True),
            lax.all_to_all(acc[None], "tp", split_axis=2, concat_axis=0, tiled=True),
        )
    )
    top, total, acc = combined_all((top, total, acc), "kv", combine)
    joined = jnp.maximum(top, self_score)
    fade = jnp.exp(top - joined)
    self_weight = jnp.exp(self_score - joined)
    total = total * fade + self_weight
    acc = (
        acc * fade[:, :, None]
        + self_weight.astype(bf16).astype(f32)[:, :, None] * new_latent.astype(f32)[:, None, :]
    )
    expanded = jnp.einsum("bhk,khv->bhv", acc, own_value_up, precision=highest)
    head_out = (expanded / total[:, :, None]).astype(bf16)
    attn_part = jnp.einsum("bhv,hvd->bd", head_out, w_attn_out, preferred_element_type=f32)
    resid_mid = resid + lax.psum(attn_part, "tp")
    scaled_mid = (resid_mid * gain_mid.astype(f32)).astype(bf16)
    hidden_part = jnp.dot(scaled_mid, w_ff_in, preferred_element_type=f32)
    square_mid = jnp.sum(resid_mid * resid_mid, axis=1)
    hidden_sum, total_mid = lax.psum((hidden_part, square_mid), "kv")
    inv_mid = lax.rsqrt(total_mid / D + EPS)[:, None]
    hidden = jnp.square(jax.nn.relu(inv_mid * hidden_sum)).astype(bf16)
    out_part = jnp.dot(hidden, w_ff_out, preferred_element_type=f32)
    mixed = (resid_mid + lax.psum(out_part, "tp")).astype(bf16)
    return (mixed, new_latent, new_rope_key)


def solution(mesh):
    return jax.shard_map(
        per_device,
        mesh=mesh,
        in_specs=(
            P(None, "kv"),
            P(),
            P(None, ("kv", "tp"), None),
            P(None, ("kv", "tp"), None),
            P("kv"),
            P("kv", None),
            P("kv", None),
            P("kv", None),
            P(),
            P(),
            P(),
            P(),
            P(),
            P(),
            P("tp", None, "kv"),
            P("kv"),
            P("kv", "tp"),
            P("tp", "kv"),
        ),
        out_specs=(P(None, "kv"), P(), P()),
        check_vma=False,
    )
```

profile of v0, /device:TPU:0, one launch (start us, length us, event | category | flops | bytes accessed | tf_op | source)
XLA Modules:
  0.0 218.2 jit_solution(16655276583001931939)
XLA Ops:
  7.2 0.8 convert_element_type.75
  8.0 0.8 fusion.23
  8.8 0.7 convert_element_type.68
  9.5 0.7 broadcast_compare_fusion
  10.2 0.7 convert_element_type.70
  10.9 0.9 fusion.41
  11.7 1.1 fusion.43
  12.8 1.2 fusion.45
  14.0 30.8 %all-reduce = (f32[16,512]{1,0:T(8,128)S(1)}, f32[16]{0:T(128)S(1)}, f32[16,256]{1,0:T(8,128)S(1)}, f32[16,32]{1,0:T(8,128)S(1)}) all-reduce(f32[16,512]{1,0:T(8,128)S(1)} %fusion.45, f32[16]{0:T(128)S(1)} %fusion.23, f32[16,256]{1,0:T(8,128)S(1)} %fusion.43, f32[16,32]{1,0:T(8,128)S(1)} %fusion.41), channel_id=1, replica_groups=mesh['kv'=8,'tp'=4] {'kv'}, use_global_device_ids=true, to_apply=%region_2.0 | all-reduce | flops 12816 | bytes 102528 | tf_op jit(solution)/shard_map/psum | solution.py:96
  44.8 0.2 multiply_reduce_fusion.1
  45.1 0.5 fusion.55
  45.6 0.7 convolution_convert_fusion
  46.5 0.1 fusion.14
  46.7 0.8 copy-done.1
  47.4 0.4 fusion.62
  47.8 0.7 copy.50
  48.5 3.7 %all-to-all-start = ((f32[1,16,16]{1,0,2:T(1,128)}), f32[1,16,16]{1,0,2:T(1,128)S(1)}, u32[]{:S(2)}, u32[]{:S(2)}) async-start(f32[1,16,16]{1,0,2:T(1,128)} %copy.50), calls=%async_computation | async-start | bytes 16384 | tf_op jit(solution)/shard_map/all_to_all | solution.py:133
  52.3 0.6 copy-done.10
  53.1 0.2 multiply_reduce_fusion.3
  53.3 0.3 convolution_bitcast_fusion
  53.6 0.7 fusion.52
  54.5 0.5 copy-done.9
  55.0 0.2 fusion.10
  55.3 0.6 copy-done.11
  56.1 0.7 copy.51
  56.8 0.8 copy.52
  57.6 4.2 %all-to-all-start.1 = ((f32[1,16,16]{1,0,2:T(1,128)}), f32[1,16,16]{1,0,2:T(1,128)S(1)}, u32[]{:S(2)}, u32[]{:S(2)}) async-start(f32[1,16,16]{1,0,2:T(1,128)} %copy.51), calls=%async_computation.1 | async-start | bytes 16384 | tf_op jit(solution)/shard_map/all_to_all | solution.py:134
  61.8 12.8 %all-gather.3 = f32[8,16,4]{1,2,0:T(4,128)S(1)} all-gather(f32[1,16,4]{1,2,0:T(4,128)S(1)} %bitcast.113), channel_id=2, replica_groups=mesh['kv'=8,'tp'=4] {'kv'}, dimensions={0}, use_global_device_ids=true | all-gather | bytes 2304 | tf_op jit(solution)/shard_map/all_gather | solution.py:13
  74.6 4.2 %all-to-all-start.2 = ((f32[1,16,16,256]{3,1,0,2:T(8,128)}), f32[1,16,16,256]{3,1,0,2:T(8,128)S(1)}, u32[]{:S(2)}, u32[]{:S(2)}) async-start(f32[1,16,16,256]{3,1,0,2:T(8,128)} %copy.52), calls=%async_computation.2 | async-start | bytes 524288 | tf_op jit(solution)/shard_map/all_to_all | solution.py:135
  78.8 12.8 %all-gather.4 = f32[8,16,4]{1,2,0:T(4,128)S(1)} all-gather(f32[1,16,4]{1,2,0:T(4,128)S(1)} %bitcast.114), channel_id=3, replica_groups=mesh['kv'=8,'tp'=4] {'kv'}, dimensions={0}, use_global_device_ids=true | all-gather | bytes 2304 | tf_op jit(solution)/shard_map/all_gather | solution.py:13
  91.8 15.1 %all-gather.2 = f32[128,4,256]{2,1,0:T(4,128)S(1)} all-gather(f32[16,4,256]{2,1,0:T(4,128)S(1)} %copy.53), channel_id=4, replica_groups=mesh['kv'=8,'tp'=4] {'kv'}, dimensions={0}, use_global_device_ids=true | all-gather | bytes 589824 | tf_op jit(solution)/shard_map/all_gather | solution.py:13
  106.8 2.5 %while.19 = (s32[]{:T(128)}, f32[16,4]{0,1:T(4,128)S(1)}, f32[16,4]{0,1:T(4,128)S(1)}, f32[16,4,256]{2,1,0:T(4,128)S(1)}, f32[8,16,4]{1,2,0:T(4,128)S(1)}, /*ind...) while((s32[]{:T(128)}, f32[16,4]{0,1:T(4,128)S(1)}, ...), condition=%wide.region_10.11_spmd, body=%wide.region_9.10_spmd.sunk | while | flops 49541 | bytes 200335 | solution.py:18
  107.0 0.1 fusion.79
  107.4 0.1 fusion.79
  107.8 0.1 fusion.79
  108.1 0.1 fusion.79
  108.5 0.1 fusion.79
  108.8 0.1 fusion.79
  109.2 0.1 fusion.79
  109.6 1.2 fusion.6
  110.8 0.2 convolution_bitcast_fusion.2
  111.0 16.5 %psum.60 = f32[16,256]{1,0:T(8,128)S(1)} all-reduce(f32[16,256]{1,0:T(8,128)S(1)} %convolution_bitcast_fusion.2), channel_id=1, replica_groups=mesh['kv'=8,'tp'=4] {'tp'}, use_global_device_ids=true, to_apply=%region_14.15 | all-reduce | flops 4096 | bytes 32768 | tf_op jit(solution)/shard_map/psum | solution.py:150
  127.6 13.6 %psum.61 = f32[16]{0:T(128)S(1)} all-reduce(f32[16]{0:T(128)S(1)} %multiply_reduce_fusion.2), channel_id=1, replica_groups=mesh['kv'=8,'tp'=4] {'kv'}, use_global_device_ids=true, to_apply=%region_16.17 | all-reduce | flops 16 | bytes 128 | tf_op jit(solution)/shard_map/psum | solution.py:154
  141.2 0.9 fusion.38
  142.2 51.4 %all-reduce.3.cloned.1.call-done = f32[16,2048]{1,0:T(8,128)} async-done(((f32[16,2048]{1,0:T(8,128)}), f32[16,2048]{1,0:T(8,128)}) %all-reduce.3.cloned.1.call-update) | async-done | bytes 131088 | tf_op jit(solution)/shard_map/psum | solution.py:154
  193.6 1.2 fusion.12
  194.8 16.0 %psum.63 = f32[16,256]{1,0:T(8,128)S(1)} all-reduce(f32[16,256]{1,0:T(8,128)S(1)} %fusion.12), channel_id=1, replica_groups=mesh['kv'=8,'tp'=4] {'tp'}, use_global_device_ids=true, to_apply=%region_18.19 | all-reduce | flops 4096 | bytes 32768 | tf_op jit(solution)/shard_map/psum | solution.py:158
  210.7 0.6 add_convert_fusion.1
  (78 shorter events, 3.2 us)
Async XLA Ops:
  7.2 38.4 %copy-start = (bf16[512,16,64]{0,2,1:T(8,128)(2,1)S(1)}, bf16[512,16,64]{0,2,1:T(8,128)(2,1)}, u32[]{:S(2)}) copy-start(bf16[512,16,64]{0,2,1:T(8,128)(2,1)} %param.29) | copy-start | bytes 3145732
  7.2 37.9 %copy-start.4 = (bf16[512,16,32]{0,2,1:T(8,128)(2,1)S(1)}, bf16[512,16,32]{0,2,1:T(8,128)(2,1)}, u32[]{:S(2)}) copy-start(bf16[512,16,32]{0,2,1:T(8,128)(2,1)} %param.30) | copy-start | bytes 1572868
  12.8 32.8 %copy-start.5 = (bf16[256,16,64]{0,2,1:T(8,128)(2,1)S(1)}, bf16[256,16,64]{0,2,1:T(8,128)(2,1)}, u32[]{:S(2)}) copy-start(bf16[256,16,64]{0,2,1:T(8,128)(2,1)} %param.32) | copy-start | bytes 1572868
  45.6 0.9 copy-start.8
  46.3 1.2 copy-start.1
  48.5 9.1 %all-to-all-start = ((f32[1,16,16]{1,0,2:T(1,128)}), f32[1,16,16]{1,0,2:T(1,128)S(1)}, u32[]{:S(2)}, u32[]{:S(2)}) async-start(f32[1,16,16]{1,0,2:T(1,128)} %copy.50), calls=%async_computation | async-start | bytes 16384 | tf_op jit(solution)/shard_map/all_to_all | solution.py:133
  52.2 0.7 copy-start.10
  54.3 0.6 copy-start.9
  55.3 0.7 copy-start.11
  57.6 17.0 %all-to-all-start.1 = ((f32[1,16,16]{1,0,2:T(1,128)}), f32[1,16,16]{1,0,2:T(1,128)S(1)}, u32[]{:S(2)}, u32[]{:S(2)}) async-start(f32[1,16,16]{1,0,2:T(1,128)} %copy.51), calls=%async_computation.1 | async-start | bytes 16384 | tf_op jit(solution)/shard_map/all_to_all | solution.py:134
  74.6 17.0 %all-to-all-start.2 = ((f32[1,16,16,256]{3,1,0,2:T(8,128)}), f32[1,16,16,256]{3,1,0,2:T(8,128)S(1)}, u32[]{:S(2)}, u32[]{:S(2)}) async-start(f32[1,16,16,256]{3,1,0,2:T(8,128)} %copy.52), calls=%async_computation.2 | async-start | bytes 524288 | tf_op jit(solution)/shard_map/all_to_all | solution.py:135
  78.8 114.8 %all-reduce.3.cloned.1.call-start = ((), (), s32[]{:S(2)}) async-start(), calls=%async_computation.3 | async-start | bytes 262144 | tf_op jit(solution)/shard_map/psum | solution.py:154
  91.7 19.0 %copy-start.7 = (bf16[4,64,256]{2,1,0:T(8,128)(2,1)S(1)}, bf16[4,64,256]{2,1,0:T(8,128)(2,1)}, u32[]{:S(2)}) copy-start(bf16[4,64,256]{2,1,0:T(8,128)(2,1)} %param.34) | copy-start | bytes 393220
  106.8 34.4 %copy-start.2 = (bf16[256,2048]{1,0:T(8,128)(2,1)S(1)}, bf16[256,2048]{1,0:T(8,128)(2,1)}, u32[]{:S(2)}) copy-start(bf16[256,2048]{1,0:T(8,128)(2,1)} %param.36) | copy-start | bytes 3145732
  106.8 20.7 %copy-start.6 = (bf16[16,256]{1,0:T(8,128)(2,1)S(1)}, bf16[16,256]{1,0:T(8,128)(2,1)}, u32[]{:S(2)}) copy-start(bf16[16,256]{1,0:T(8,128)(2,1)} %param.20) | copy-start | bytes 24580
  109.3 84.3 %copy-start.3 = (bf16[2048,256]{1,0:T(8,128)(2,1)S(1)}, bf16[2048,256]{1,0:T(8,128)(2,1)}, u32[]{:S(2)}) copy-start(bf16[2048,256]{1,0:T(8,128)(2,1)} %param.37) | copy-start | bytes 3145732
Sparse Core Ops, SparseCore 0:
  142.3 51.2 all-reduce.2
where the time goes:
time: 219 us; the launch traced here: 218 us
  blocking collectives  117 us (53%)
  waiting for transfers between devices  51.5 us (24%)
  between operations  14.2 us (6%)
  starting transfers between devices  12.1 us (6%)
  matrix products  8.74 us (4%)
  other arithmetic  7.81 us (4%)
  local copies, waits for them, and re-layouts  6.26 us (3%)
    psum x1, waiting for transfers between devices, per_device(): hidden_sum, total_mid = lax.psum((hidden_part, square_mid), 'kv')  51.4 us
    all_gather x3, blocking collectives, combined_all(): gathered = jax.tree.map(lambda a: lax.all_gather(a, axis), part)  40.6 us
    psum x1, blocking collectives, per_device(): lax.psum((part_q, part_kv, part_rope, square_in), 'kv')  30.8 us
    psum x1, blocking collectives, per_device(): resid_mid = resid + lax.psum(attn_part, 'tp')  16.5 us
    psum x1, blocking collectives, per_device(): mixed = (resid_mid + lax.psum(out_part, 'tp')).astype(bf16)  16 us
    psum x1, blocking collectives, per_device(): hidden_sum, total_mid = lax.psum((hidden_part, square_mid), 'kv')  13.6 us
  transfers between devices with their start and end apart: 4, of which 1 were waited for; matrix products, arithmetic and copies ran while one was open for 2% of the time, Pallas kernels for 0%

commit v1 on v0

--- a/solution.py
+++ b/solution.py
@@ -155,7 +155,7 @@
     inv_mid = lax.rsqrt(total_mid / D + EPS)[:, None]
     hidden = jnp.square(jax.nn.relu(inv_mid * hidden_sum)).astype(bf16)
     out_part = jnp.dot(hidden, w_ff_out, preferred_element_type=f32)
-    mixed = (resid_mid + lax.psum(out_part, "tp")).astype(bf16)
+    mixed = (resid_mid + jnp.sum(lax.all_gather(out_part, "tp"), axis=0)).astype(bf16)
     return (mixed, new_latent, new_rope_key)
 
 

time: 219 us -> 211 us (0.963)
  blocking collectives: 117 us -> 110 us
    psum x1 -> x0, blocking collectives: 16 us -> none  [per_device(): mixed = (resid_mid + lax.psum(out_part, 'tp')).astype(bf16)]
    all_gather x0 -> x1, blocking collectives: none -> 8.19 us  [per_device(): lax.all_gather(out_part, 'tp')]
where the time goes in v1:
time: 211 us; the launch traced here: 210 us
  blocking collectives  110 us (52%)
  waiting for transfers between devices  51.5 us (24%)
  between operations  14.3 us (7%)
  starting transfers between devices  12.1 us (6%)
  matrix products  8.74 us (4%)
  other arithmetic  7.82 us (4%)
  local copies, waits for them, and re-layouts  6.26 us (3%)
    psum x1, waiting for transfers between devices, per_device(): hidden_sum, total_mid = lax.psum((hidden_part, square_mid), 'kv')  51.4 us
    all_gather x3, blocking collectives, combined_all(): gathered = jax.tree.map(lambda a: lax.all_gather(a, axis), part)  40.6 us
    psum x1, blocking collectives, per_device(): lax.psum((part_q, part_kv, part_rope, square_in), 'kv')  30.8 us
    psum x1, blocking collectives, per_device(): resid_mid = resid + lax.psum(attn_part, 'tp')  16.5 us
    psum x1, blocking collectives, per_device(): hidden_sum, total_mid = lax.psum((hidden_part, square_mid), 'kv')  13.6 us
    all_gather x1, blocking collectives, per_device(): lax.all_gather(out_part, 'tp')  8.19 us
  transfers between devices with their start and end apart: 4, of which 1 were waited for; matrix products, arithmetic and copies ran while one was open for 2% of the time, Pallas kernels for 0%

profile of v1, /device:TPU:0, one launch (start us, length us, event | category | flops | bytes accessed | tf_op | source)
XLA Modules:
  0.0 210.4 jit_solution(328475554746534807)
XLA Ops:
  7.2 0.8 convert_element_type.75
  8.0 0.8 fusion.23
  8.8 0.7 convert_element_type.68
  9.5 0.7 broadcast_compare_fusion
  10.2 0.7 convert_element_type.70
  10.9 0.9 fusion.41
  11.7 1.1 fusion.43
  12.8 1.2 fusion.45
  14.0 30.8 %all-reduce = (f32[16,512]{1,0:T(8,128)S(1)}, f32[16]{0:T(128)S(1)}, f32[16,256]{1,0:T(8,128)S(1)}, f32[16,32]{1,0:T(8,128)S(1)}) all-reduce(f32[16,512]{1,0:T(8,128)S(1)} %fusion.45, f32[16]{0:T(128)S(1)} %fusion.23, f32[16,256]{1,0:T(8,128)S(1)} %fusion.43, f32[16,32]{1,0:T(8,128)S(1)} %fusion.41), channel_id=1, replica_groups=mesh['kv'=8,'tp'=4] {'kv'}, use_global_device_ids=true, to_apply=%region_2.0 | all-reduce | flops 12816 | bytes 102528 | tf_op jit(solution)/shard_map/psum | solution.py:96
  44.8 0.2 multiply_reduce_fusion.1
  45.1 0.5 fusion.55
  45.6 0.7 convolution_convert_fusion
  46.5 0.1 fusion.14
  46.7 0.8 copy-done.1
  47.4 0.4 fusion.62
  47.8 0.7 copy.50
  48.5 3.7 %all-to-all-start = ((f32[1,16,16]{1,0,2:T(1,128)}), f32[1,16,16]{1,0,2:T(1,128)S(1)}, u32[]{:S(2)}, u32[]{:S(2)}) async-start(f32[1,16,16]{1,0,2:T(1,128)} %copy.50), calls=%async_computation | async-start | bytes 16384 | tf_op jit(solution)/shard_map/all_to_all | solution.py:133
  52.3 0.6 copy-done.10
  53.1 0.2 multiply_reduce_fusion.3
  53.3 0.3 convolution_bitcast_fusion
  53.6 0.7 fusion.52
  54.5 0.5 copy-done.9
  55.0 0.2 fusion.10
  55.3 0.6 copy-done.11
  56.1 0.7 copy.51
  56.8 0.8 copy.52
  57.6 4.2 %all-to-all-start.1 = ((f32[1,16,16]{1,0,2:T(1,128)}), f32[1,16,16]{1,0,2:T(1,128)S(1)}, u32[]{:S(2)}, u32[]{:S(2)}) async-start(f32[1,16,16]{1,0,2:T(1,128)} %copy.51), calls=%async_computation.1 | async-start | bytes 16384 | tf_op jit(solution)/shard_map/all_to_all | solution.py:134
  61.8 12.8 %all-gather.4 = f32[8,16,4]{1,2,0:T(4,128)S(1)} all-gather(f32[1,16,4]{1,2,0:T(4,128)S(1)} %bitcast.115), channel_id=2, replica_groups=mesh['kv'=8,'tp'=4] {'kv'}, dimensions={0}, use_global_device_ids=true | all-gather | bytes 2304 | tf_op jit(solution)/shard_map/all_gather | solution.py:13
  74.6 4.2 %all-to-all-start.2 = ((f32[1,16,16,256]{3,1,0,2:T(8,128)}), f32[1,16,16,256]{3,1,0,2:T(8,128)S(1)}, u32[]{:S(2)}, u32[]{:S(2)}) async-start(f32[1,16,16,256]{3,1,0,2:T(8,128)} %copy.52), calls=%async_computation.2 | async-start | bytes 524288 | tf_op jit(solution)/shard_map/all_to_all | solution.py:135
  78.8 12.8 %all-gather.5 = f32[8,16,4]{1,2,0:T(4,128)S(1)} all-gather(f32[1,16,4]{1,2,0:T(4,128)S(1)} %bitcast.116), channel_id=3, replica_groups=mesh['kv'=8,'tp'=4] {'kv'}, dimensions={0}, use_global_device_ids=true | all-gather | bytes 2304 | tf_op jit(solution)/shard_map/all_gather | solution.py:13
  91.8 15.1 %all-gather.2 = f32[128,4,256]{2,1,0:T(4,128)S(1)} all-gather(f32[16,4,256]{2,1,0:T(4,128)S(1)} %copy.53), channel_id=4, replica_groups=mesh['kv'=8,'tp'=4] {'kv'}, dimensions={0}, use_global_device_ids=true | all-gather | bytes 589824 | tf_op jit(solution)/shard_map/all_gather | solution.py:13
  106.8 2.5 %while.19 = (s32[]{:T(128)}, f32[16,4]{0,1:T(4,128)S(1)}, f32[16,4]{0,1:T(4,128)S(1)}, f32[16,4,256]{2,1,0:T(4,128)S(1)}, f32[8,16,4]{1,2,0:T(4,128)S(1)}, /*ind...) while((s32[]{:T(128)}, f32[16,4]{0,1:T(4,128)S(1)}, ...), condition=%wide.region_10.11_spmd, body=%wide.region_9.10_spmd.sunk | while | flops 49541 | bytes 200335 | solution.py:18
  107.0 0.1 fusion.79
  107.4 0.1 fusion.79
  107.8 0.1 fusion.79
  108.1 0.1 fusion.79
  108.5 0.1 fusion.79
  108.8 0.1 fusion.79
  109.2 0.1 fusion.79
  109.6 1.2 fusion.6
  110.8 0.2 convolution_bitcast_fusion.2
  111.0 16.5 %psum.53 = f32[16,256]{1,0:T(8,128)S(1)} all-reduce(f32[16,256]{1,0:T(8,128)S(1)} %convolution_bitcast_fusion.2), channel_id=1, replica_groups=mesh['kv'=8,'tp'=4] {'tp'}, use_global_device_ids=true, to_apply=%region_14.15 | all-reduce | flops 4096 | bytes 32768 | tf_op jit(solution)/shard_map/psum | solution.py:150
  127.6 13.6 %psum.54 = f32[16]{0:T(128)S(1)} all-reduce(f32[16]{0:T(128)S(1)} %multiply_reduce_fusion.2), channel_id=1, replica_groups=mesh['kv'=8,'tp'=4] {'kv'}, use_global_device_ids=true, to_apply=%region_16.17 | all-reduce | flops 16 | bytes 128 | tf_op jit(solution)/shard_map/psum | solution.py:154
  141.2 0.9 fusion.38
  142.2 51.4 %all-reduce.3.cloned.1.call-done = f32[16,2048]{1,0:T(8,128)} async-done(((f32[16,2048]{1,0:T(8,128)}), f32[16,2048]{1,0:T(8,128)}) %all-reduce.3.cloned.1.call-update) | async-done | bytes 131088 | tf_op jit(solution)/shard_map/psum | solution.py:154
  193.6 1.2 fusion.12
  194.8 8.2 %all-gather.3 = f32[64,256]{1,0:T(8,128)S(1)} all-gather(f32[16,256]{1,0:T(8,128)S(1)} %fusion.12), channel_id=5, replica_groups=mesh['kv'=8,'tp'=4] {'tp'}, dimensions={0}, use_global_device_ids=true | all-gather | bytes 81920 | tf_op jit(solution)/shard_map/all_gather | solution.py:158
  203.0 0.6 add_convert_fusion.1
  (79 shorter events, 3.2 us)
Async XLA Ops:
  7.2 38.4 %copy-start = (bf16[512,16,64]{0,2,1:T(8,128)(2,1)S(1)}, bf16[512,16,64]{0,2,1:T(8,128)(2,1)}, u32[]{:S(2)}) copy-start(bf16[512,16,64]{0,2,1:T(8,128)(2,1)} %param.29) | copy-start | bytes 3145732
  7.2 37.9 %copy-start.4 = (bf16[512,16,32]{0,2,1:T(8,128)(2,1)S(1)}, bf16[512,16,32]{0,2,1:T(8,128)(2,1)}, u32[]{:S(2)}) copy-start(bf16[512,16,32]{0,2,1:T(8,128)(2,1)} %param.30) | copy-start | bytes 1572868
  12.8 32.8 %copy-start.5 = (bf16[256,16,64]{0,2,1:T(8,128)(2,1)S(1)}, bf16[256,16,64]{0,2,1:T(8,128)(2,1)}, u32[]{:S(2)}) copy-start(bf16[256,16,64]{0,2,1:T(8,128)(2,1)} %param.32) | copy-start | bytes 1572868
  45.6 0.9 copy-start.8
  46.3 1.2 copy-start.1
  48.5 9.1 %all-to-all-start = ((f32[1,16,16]{1,0,2:T(1,128)}), f32[1,16,16]{1,0,2:T(1,128)S(1)}, u32[]{:S(2)}, u32[]{:S(2)}) async-start(f32[1,16,16]{1,0,2:T(1,128)} %copy.50), calls=%async_computation | async-start | bytes 16384 | tf_op jit(solution)/shard_map/all_to_all | solution.py:133
  52.2 0.7 copy-start.10
  54.3 0.6 copy-start.9
  55.3 0.7 copy-start.11
  57.6 17.0 %all-to-all-start.1 = ((f32[1,16,16]{1,0,2:T(1,128)}), f32[1,16,16]{1,0,2:T(1,128)S(1)}, u32[]{:S(2)}, u32[]{:S(2)}) async-start(f32[1,16,16]{1,0,2:T(1,128)} %copy.51), calls=%async_computation.1 | async-start | bytes 16384 | tf_op jit(solution)/shard_map/all_to_all | solution.py:134
  74.6 17.0 %all-to-all-start.2 = ((f32[1,16,16,256]{3,1,0,2:T(8,128)}), f32[1,16,16,256]{3,1,0,2:T(8,128)S(1)}, u32[]{:S(2)}, u32[]{:S(2)}) async-start(f32[1,16,16,256]{3,1,0,2:T(8,128)} %copy.52), calls=%async_computation.2 | async-start | bytes 524288 | tf_op jit(solution)/shard_map/all_to_all | solution.py:135
  78.8 114.8 %all-reduce.3.cloned.1.call-start = ((), (), s32[]{:S(2)}) async-start(), calls=%async_computation.3 | async-start | bytes 262144 | tf_op jit(solution)/shard_map/psum | solution.py:154
  91.7 19.0 %copy-start.7 = (bf16[4,64,256]{2,1,0:T(8,128)(2,1)S(1)}, bf16[4,64,256]{2,1,0:T(8,128)(2,1)}, u32[]{:S(2)}) copy-start(bf16[4,64,256]{2,1,0:T(8,128)(2,1)} %param.34) | copy-start | bytes 393220
  106.8 34.4 %copy-start.2 = (bf16[256,2048]{1,0:T(8,128)(2,1)S(1)}, bf16[256,2048]{1,0:T(8,128)(2,1)}, u32[]{:S(2)}) copy-start(bf16[256,2048]{1,0:T(8,128)(2,1)} %param.36) | copy-start | bytes 3145732
  106.8 20.7 %copy-start.6 = (bf16[16,256]{1,0:T(8,128)(2,1)S(1)}, bf16[16,256]{1,0:T(8,128)(2,1)}, u32[]{:S(2)}) copy-start(bf16[16,256]{1,0:T(8,128)(2,1)} %param.20) | copy-start | bytes 24580
  109.3 84.3 %copy-start.3 = (bf16[2048,256]{1,0:T(8,128)(2,1)S(1)}, bf16[2048,256]{1,0:T(8,128)(2,1)}, u32[]{:S(2)}) copy-start(bf16[2048,256]{1,0:T(8,128)(2,1)} %param.37) | copy-start | bytes 3145732
Sparse Core Ops, SparseCore 0:
  142.3 51.2 all-reduce.2
